TPU v7x, 32 devices: a whole 2x2x4 slice. The times are simulated.
32 devices in a mesh: sp: 4 (over z), tp: 8 (over y, x, core).
Axes of the slice: x: 2, y: 2, z: 4, core: 2. Of those that a mesh axis runs over, the one named last changes fastest.
Arguments:
- stream: bfloat16 [1024, 4096], P('sp', 'tp'), may hold values from -80 to 80
- norm_gain: bfloat16 [3, 4096], replicated, may hold values from 0.099609375 to 1.8984375
- value_weight: bfloat16 [3, 2048, 4096], P(None, 'tp'), may hold values from -0.09375 to 0.09375
- gate_weight: bfloat16 [3, 2048, 4096], P(None, 'tp'), may hold values from -0.09375 to 0.09375
- kernel: float32 [3, 31, 2048], P(None, None, 'tp'), may hold values from -8 to 8
- kernel_bias: float32 [3, 2048], P(None, 'tp'), may hold values from -3 to 3
- chan_gain: float32 [3, 2048], P(None, 'tp'), may hold values from 0.1 to 1.9
- chan_shift: float32 [3, 2048], P(None, 'tp'), may hold values from -3 to 3
- out_weight: bfloat16 [3, 2048, 4096], P(None, None, 'tp'), may hold values from -0.125 to 0.125
Outputs:
- result: bfloat16 [1024, 4096], P('sp', 'tp')
All inputs are finite; a program needn't handle non-finite values.
Results may differ from a plain program's by a relative error of at most 0.012.
Values may be sent and summed in bfloat16 or wider, within the bound.
A program may use at most 64 MiB of HBM per device.

v0:
```python
import jax
import jax.numpy as jnp
from jax import lax
from jax.sharding import PartitionSpec as P

EPSILON = 1e-06


def passed_along(shard, axis, by):
    count = lax.axis_size(axis)
    pairs = [(i, i + by) for i in range(count) if 0 <= i + by < count]
    return lax.ppermute(shard, axis, pairs)


def against(left, right):
    return lax.dot_general(
        left, right, (((1,), (1,)), ((), ())), preferred_element_type=jnp.float32
    )


def on_device(
    stream,
    norm_gain,
    value_weight,
    gate_weight,
    kernel,
    kernel_bias,
    chan_gain,
    chan_shift,
    out_weight,
):
    layer_count = kernel.shape[0]
    reach_back = kernel.shape[1] - 1
    local_width = stream.shape[1]
    channels = kernel.shape[2] * lax.axis_size("tp")
    current = stream
    for layer_at in range(layer_count):
        gain_row = norm_gain[layer_at].astype(jnp.float32)
        value_matrix = value_weight[layer_at]
        gate_matrix = gate_weight[layer_at]
        row_count = current.shape[0]
        whole_rows = lax.all_gather(current, "tp", axis=1, tiled=True)
        whole_float = whole_rows.astype(jnp.float32)
        scale_row = lax.rsqrt(jnp.mean(whole_float * whole_float, axis=1, keepdims=True) + EPSILON)
        normed = (whole_float * scale_row * gain_row[None, :]).astype(jnp.bfloat16)
        value_part = against(normed, value_matrix)
        gate_part = against(normed, gate_matrix)
        gated_rows = (value_part * jax.nn.sigmoid(gate_part)).astype(jnp.bfloat16)
        earlier_taps = passed_along(gated_rows[row_count - reach_back :], "sp", 1)
        padded = jnp.concatenate([earlier_taps, gated_rows], axis=0)
        out_rows = padded.shape[0] - reach_back
        kernel_now = kernel[layer_at]
        convolved = jnp.broadcast_to(
            kernel_bias[layer_at][None, :], (out_rows, kernel_now.shape[1])
        )
        for tap_at in range(reach_back + 1):
            convolved = convolved + kernel_now[tap_at][None, :] * padded[
                tap_at : tap_at + out_rows
            ].astype(jnp.float32)
        totals = lax.psum(
            (jnp.sum(convolved, axis=1), jnp.sum(convolved * convolved, axis=1)), "tp"
        )
        centre = totals[0] / channels
        spread = totals[1] / channels - centre * centre
        normal_out = (convolved - centre[:, None]) * lax.rsqrt(spread + EPSILON)[
            :, None
        ] * chan_gain[layer_at][None, :] + chan_shift[layer_at][None, :]
        hidden = jax.nn.silu(normal_out).astype(jnp.bfloat16)
        out_matrix = out_weight[layer_at]

        def project_out(running, block_in, offset_at, out_matrix=out_matrix):
            return jnp.dot(block_in, out_matrix, preferred_element_type=jnp.float32)

        projected = project_out(
            jnp.zeros((out_rows, local_width), jnp.float32),
            lax.all_gather(hidden, "tp", axis=1, tiled=True),
            jnp.int32(0),
        )
        current = (current.astype(jnp.float32) + projected).astype(jnp.bfloat16)
    return current


def solution(mesh):
    return jax.shard_map(
        on_device,
        mesh=mesh,
        in_specs=(
            P("sp", "tp"),
            P(),
            P(None, "tp", None),
            P(None, "tp", None),
            P(None, None, "tp"),
            P(None, "tp"),
            P(None, "tp"),
            P(None, "tp"),
            P(None, None, "tp"),
        ),
        out_specs=P("sp", "tp"),
        check_vma=False,
    )
```

profile of v0, /device:TPU:25, one launch (start us, length us, event | category | flops | bytes accessed | tf_op | source)
XLA Modules:
  0.0 265.4 jit_solution(3278399664090631594)
XLA Ops:
  6.5 0.0 all-gather.7.cloned.1.call-start
  6.5 0.7 all-gather.7.cloned.1.call-update
  7.3 0.0 all-gather.9.cloned.1.call-start
  7.3 0.8 fusion.211
  8.1 0.8 fusion.209
  8.9 1.0 fusion.208
  9.9 1.1 fusion.207
  11.1 0.9 slice_convert_fusion
  12.0 26.8 %all-gather.7.cloned.1.call-done = bf16[256,4096]{1,0:T(8,128)(2,1)} async-done(((bf16[256,512]{1,0:T(8,128)(2,1)}), bf16[256,4096]{1,0:T(8,128)(2,1)}) %all-gather.7.cloned.1.call-update) | async-done | bytes 2097168 | tf_op jit(solution)/shard_map/all_gather | solution.py:42
  38.7 2.1 fusion
  40.8 0.0 copy-start
  40.8 3.2 %fusion.96 = f32[256,256]{1,0:T(8,128)S(1)} fusion(bf16[3,256,4096]{2,1,0:T(8,128)(2,1)} %param.12, bf16[256,4096]{1,0:T(8,128)(2,1)} %all-gather.7.cloned.1.call-done, f32[4096]{0:T(1024)S(1)} %bitcast.187, f32[256]{0:T(256)S(1)} %add_rsqrt_fusion.5), kind=kOutput, calls=%fused_computation.149 | convolution fusion | flops 541261824 | bytes 4473856 | tf_op jit(solution)/shard_map/dot_general | solution.py:16
  44.0 0.0 copy-done
  44.0 0.0 copy-start.7
  44.0 0.0 copy-start.3
  44.0 2.5 fusion.105
  46.5 0.0 copy-start.6
  46.5 1.4 collective-permute-start
  48.0 0.0 copy-done.7
  48.0 3.2 %collective-permute-done = bf16[30,256]{1,0:T(8,128)(2,1)S(1)} collective-permute-done((bf16[30,256]{1,0:T(8,128)(2,1)S(1)}, bf16[30,256]{1,0:T(8,128)(2,1)S(1)}, u32[]{:S(2)}, u32[]{:S(2)}) %collective-permute-start) | collective-permute-done | bytes 15392 | tf_op jit(solution)/shard_map/ppermute | solution.py:12
  51.1 1.2 fusion.203
  52.3 12.6 %all-reduce.2 = (f32[256]{0:T(256)S(1)}, f32[256]{0:T(256)S(1)}) all-reduce(f32[256]{0:T(256)S(1)} %get-tuple-element.10, f32[256]{0:T(256)S(1)} %get-tuple-element.9), channel_id=1, replica_groups=mesh['sp'=4,'tp'=8] {'tp'}, use_global_device_ids=true, to_apply=%region_4.0 | all-reduce | flops 512 | bytes 4096 | tf_op jit(solution)/shard_map/psum | solution.py:60
  64.9 0.9 multiply_convert_fusion.2
  65.8 0.0 all-gather.9.cloned.1.call-update
  65.8 0.0 all-gather.11.cloned.1.call-start
  65.8 24.1 %all-gather.9.cloned.1.call-done = bf16[256,2048]{1,0:T(8,128)(2,1)} async-done(((bf16[256,256]{1,0:T(8,128)(2,1)}), bf16[256,2048]{1,0:T(8,128)(2,1)}) %all-gather.9.cloned.1.call-update) | async-done | bytes 1048592 | tf_op jit(solution)/shard_map/all_gather | solution.py:76
  90.0 0.0 copy-done.3
  90.0 3.3 %fusion.51 = bf16[256,512]{1,0:T(8,128)(2,1)} fusion(bf16[256,2048]{1,0:T(8,128)(2,1)} %all-gather.9.cloned.1.call-done, bf16[3,2048,512]{2,1,0:T(8,128)(2,1)} %param.17, bf16[256,512]{1,0:T(8,128)(2,1)S(1)} %copy-done.3), kind=kOutput, calls=%fused_computation.134 | convolution fusion | flops 537264128 | bytes 3670016 | tf_op jit(solution)/shard_map/dot_general | solution.py:72
  93.3 0.0 all-gather.11.cloned.1.call-update
  93.3 0.0 all-gather.13.cloned.1.call-start
  93.4 0.0 copy-done.6
  93.4 28.2 %all-gather.11.cloned.1.call-done = bf16[256,4096]{1,0:T(8,128)(2,1)} async-done(((bf16[256,512]{1,0:T(8,128)(2,1)}), bf16[256,4096]{1,0:T(8,128)(2,1)}) %all-gather.11.cloned.1.call-update) | async-done | bytes 2097168 | tf_op jit(solution)/shard_map/all_gather | solution.py:42
  121.6 2.1 fusion.3
  123.7 3.2 %fusion.93 = f32[256,256]{1,0:T(8,128)S(1)} fusion(bf16[3,256,4096]{2,1,0:T(8,128)(2,1)} %param.12, bf16[256,4096]{1,0:T(8,128)(2,1)} %all-gather.11.cloned.1.call-done, f32[4096]{0:T(1024)S(1)} %bitcast.185, f32[256]{0:T(256)S(1)} %add_rsqrt_fusion.3), kind=kOutput, calls=%fused_computation.148 | convolution fusion | flops 541261824 | bytes 4473856 | tf_op jit(solution)/shard_map/dot_general | solution.py:16
  126.8 0.0 copy-done.1
  126.8 0.0 copy-start.4
  126.9 2.4 fusion.102
  129.3 1.3 collective-permute-start.1
  130.7 3.2 %collective-permute-done.1 = bf16[30,256]{1,0:T(8,128)(2,1)S(1)} collective-permute-done((bf16[30,256]{1,0:T(8,128)(2,1)S(1)}, bf16[30,256]{1,0:T(8,128)(2,1)S(1)}, u32[]{:S(2)}, u32[]{:S(2)}) %collective-permute-start.1) | collective-permute-done | bytes 15392 | tf_op jit(solution)/shard_map/ppermute | solution.py:12
  133.8 1.2 fusion.202
  135.0 12.6 %all-reduce.1 = (f32[256]{0:T(256)S(1)}, f32[256]{0:T(256)S(1)}) all-reduce(f32[256]{0:T(256)S(1)} %get-tuple-element.8, f32[256]{0:T(256)S(1)} %get-tuple-element.7), channel_id=1, replica_groups=mesh['sp'=4,'tp'=8] {'tp'}, use_global_device_ids=true, to_apply=%region_9.10 | all-reduce | flops 512 | bytes 4096 | tf_op jit(solution)/shard_map/psum | solution.py:60
  147.6 0.8 multiply_convert_fusion.1
  148.4 0.0 all-gather.13.cloned.1.call-update
  148.4 0.0 all-gather.15.cloned.1.call-start
  148.5 24.1 %all-gather.13.cloned.1.call-done = bf16[256,2048]{1,0:T(8,128)(2,1)} async-done(((bf16[256,256]{1,0:T(8,128)(2,1)}), bf16[256,2048]{1,0:T(8,128)(2,1)}) %all-gather.13.cloned.1.call-update) | async-done | bytes 1048592 | tf_op jit(solution)/shard_map/all_gather | solution.py:76
  172.6 0.0 copy-done.4
  172.6 3.3 %fusion.48 = bf16[256,512]{1,0:T(8,128)(2,1)} fusion(bf16[256,2048]{1,0:T(8,128)(2,1)} %all-gather.13.cloned.1.call-done, bf16[3,2048,512]{2,1,0:T(8,128)(2,1)} %param.17, bf16[256,512]{1,0:T(8,128)(2,1)S(1)} %copy-done.4), kind=kOutput, calls=%fused_computation.133 | convolution fusion | flops 537264128 | bytes 3670016 | tf_op jit(solution)/shard_map/dot_general | solution.py:72
  175.9 0.0 all-gather.15.cloned.1.call-update
  176.0 0.0 all-gather.17.cloned.1.call-start
  176.0 28.2 %all-gather.15.cloned.1.call-done = bf16[256,4096]{1,0:T(8,128)(2,1)} async-done(((bf16[256,512]{1,0:T(8,128)(2,1)}), bf16[256,4096]{1,0:T(8,128)(2,1)}) %all-gather.15.cloned.1.call-update) | async-done | bytes 2097168 | tf_op jit(solution)/shard_map/all_gather | solution.py:42
  204.2 2.1 fusion.6
  206.3 3.2 %fusion.90 = f32[256,256]{1,0:T(8,128)S(1)} fusion(bf16[3,256,4096]{2,1,0:T(8,128)(2,1)} %param.12, bf16[256,4096]{1,0:T(8,128)(2,1)} %all-gather.15.cloned.1.call-done, f32[4096]{0:T(1024)S(1)} %bitcast.183, f32[256]{0:T(256)S(1)} %add_rsqrt_fusion.1), kind=kOutput, calls=%fused_computation.147 | convolution fusion | flops 541261824 | bytes 4473856 | tf_op jit(solution)/shard_map/dot_general | solution.py:16
  209.5 0.0 copy-done.2
  209.5 0.0 copy-start.5
  209.5 2.5 fusion.99
  212.0 1.3 collective-permute-start.2
  213.3 3.2 %collective-permute-done.2 = bf16[30,256]{1,0:T(8,128)(2,1)S(1)} collective-permute-done((bf16[30,256]{1,0:T(8,128)(2,1)S(1)}, bf16[30,256]{1,0:T(8,128)(2,1)S(1)}, u32[]{:S(2)}, u32[]{:S(2)}) %collective-permute-start.2) | collective-permute-done | bytes 15392 | tf_op jit(solution)/shard_map/ppermute | solution.py:12
  216.5 1.2 fusion.201
  217.7 12.6 %all-reduce = (f32[256]{0:T(256)S(1)}, f32[256]{0:T(256)S(1)}) all-reduce(f32[256]{0:T(256)S(1)} %get-tuple-element.6, f32[256]{0:T(256)S(1)} %get-tuple-element.5), channel_id=1, replica_groups=mesh['sp'=4,'tp'=8] {'tp'}, use_global_device_ids=true, to_apply=%region_14.15 | all-reduce | flops 512 | bytes 4096 | tf_op jit(solution)/shard_map/psum | solution.py:60
  230.2 0.8 multiply_convert_fusion
  231.1 0.0 all-gather.17.cloned.1.call-update
  231.1 24.2 %all-gather.17.cloned.1.call-done = bf16[256,2048]{1,0:T(8,128)(2,1)} async-done(((bf16[256,256]{1,0:T(8,128)(2,1)}), bf16[256,2048]{1,0:T(8,128)(2,1)}) %all-gather.17.cloned.1.call-update) | async-done | bytes 1048592 | tf_op jit(solution)/shard_map/all_gather | solution.py:76
  255.3 0.0 copy-done.5
  255.3 3.3 %fusion.45 = bf16[256,512]{1,0:T(8,128)(2,1)} fusion(bf16[256,2048]{1,0:T(8,128)(2,1)} %all-gather.17.cloned.1.call-done, bf16[3,2048,512]{2,1,0:T(8,128)(2,1)} %param.17, bf16[256,512]{1,0:T(8,128)(2,1)S(1)} %copy-done.5), kind=kOutput, calls=%fused_computation.132 | convolution fusion | flops 537264128 | bytes 3670016 | tf_op jit(solution)/shard_map/dot_general | solution.py:72
  (15 shorter events, 0.1 us)
Async XLA Ops:
  6.5 32.2 %all-gather.7.cloned.1.call-start = ((), (), s32[]{:S(2)}) async-start(), calls=%async_computation | async-start | bytes 2359296 | tf_op jit(solution)/shard_map/all_gather | solution.py:42
  7.3 82.7 %all-gather.9.cloned.1.call-start = ((), (), s32[]{:S(2)}) async-start(), calls=%async_computation.1 | async-start | bytes 1179648 | tf_op jit(solution)/shard_map/all_gather | solution.py:76
  40.8 3.2 %copy-start = (bf16[256,4096]{1,0:T(8,128)(2,1)S(1)}, bf16[256,4096]{1,0:T(8,128)(2,1)}, u32[]{:S(2)}) copy-start(bf16[256,4096]{1,0:T(8,128)(2,1)} %all-gather.7.cloned.1.call-done) | copy-start | bytes 6291460
  44.0 3.9 %copy-start.7 = (f32[3,256]{1,0:T(4,128)S(1)}, f32[3,256]{1,0:T(4,128)}, u32[]{:S(2)}) copy-start(f32[3,256]{1,0:T(4,128)} %param.16) | copy-start | bytes 9220
  44.0 45.9 %copy-start.3 = (bf16[256,512]{1,0:T(8,128)(2,1)S(1)}, bf16[256,512]{1,0:T(8,128)(2,1)}, u32[]{:S(2)}) copy-start(bf16[256,512]{1,0:T(8,128)(2,1)} %param.9) | copy-start | bytes 786436
  46.5 46.9 %copy-start.6 = (f32[3,31,256]{2,1,0:T(8,128)S(1)}, f32[3,31,256]{2,1,0:T(8,128)}, u32[]{:S(2)}) copy-start(f32[3,31,256]{2,1,0:T(8,128)} %param.13) | copy-start | bytes 285700
  46.5 4.6 %collective-permute-start = (bf16[30,256]{1,0:T(8,128)(2,1)S(1)}, bf16[30,256]{1,0:T(8,128)(2,1)S(1)}, u32[]{:S(2)}, u32[]{:S(2)}) collective-permute-start(bf16[30,256]{1,0:T(8,128)(2,1)S(1)} %slice.1017), channel_id=1, source_target_pairs={{0,8},{8,16},{16,24},{1,9},{9,17},{17,25},{2,10},{10,18},{18,26},{... | collective-permute-start | bytes 46088 | tf_op jit(solution)/shard_map/ppermute | solution.py:12
  65.8 55.8 %all-gather.11.cloned.1.call-start = ((), (), s32[]{:S(2)}) async-start(), calls=%async_computation.2 | async-start | bytes 2359296 | tf_op jit(solution)/shard_map/all_gather | solution.py:42
  93.3 79.3 %all-gather.13.cloned.1.call-start = ((), (), s32[]{:S(2)}) async-start(), calls=%async_computation.3 | async-start | bytes 1179648 | tf_op jit(solution)/shard_map/all_gather | solution.py:76
  123.7 3.2 %copy-start.1 = (bf16[256,4096]{1,0:T(8,128)(2,1)S(1)}, bf16[256,4096]{1,0:T(8,128)(2,1)}, u32[]{:S(2)}) copy-start(bf16[256,4096]{1,0:T(8,128)(2,1)} %all-gather.11.cloned.1.call-done) | copy-start | bytes 6291460
  126.8 45.8 %copy-start.4 = (bf16[256,512]{1,0:T(8,128)(2,1)S(1)}, bf16[256,512]{1,0:T(8,128)(2,1)}, u32[]{:S(2)}) copy-start(bf16[256,512]{1,0:T(8,128)(2,1)} %fusion.51) | copy-start | bytes 786436
  129.3 4.5 %collective-permute-start.1 = (bf16[30,256]{1,0:T(8,128)(2,1)S(1)}, bf16[30,256]{1,0:T(8,128)(2,1)S(1)}, u32[]{:S(2)}, u32[]{:S(2)}) collective-permute-start(bf16[30,256]{1,0:T(8,128)(2,1)S(1)} %slice.1076), channel_id=1, source_target_pairs={{0,8},{8,16},{16,24},{1,9},{9,17},{17,25},{2,10},{10,18},{18,26},{... | collective-permute-start | bytes 46088 | tf_op jit(solution)/shard_map/ppermute | solution.py:12
  148.4 55.8 %all-gather.15.cloned.1.call-start = ((), (), s32[]{:S(2)}) async-start(), calls=%async_computation.4 | async-start | bytes 2359296 | tf_op jit(solution)/shard_map/all_gather | solution.py:42
  176.0 79.3 %all-gather.17.cloned.1.call-start = ((), (), s32[]{:S(2)}) async-start(), calls=%async_computation.5 | async-start | bytes 1179648 | tf_op jit(solution)/shard_map/all_gather | solution.py:76
  206.3 3.2 %copy-start.2 = (bf16[256,4096]{1,0:T(8,128)(2,1)S(1)}, bf16[256,4096]{1,0:T(8,128)(2,1)}, u32[]{:S(2)}) copy-start(bf16[256,4096]{1,0:T(8,128)(2,1)} %all-gather.15.cloned.1.call-done) | copy-start | bytes 6291460
  209.5 45.8 %copy-start.5 = (bf16[256,512]{1,0:T(8,128)(2,1)S(1)}, bf16[256,512]{1,0:T(8,128)(2,1)}, u32[]{:S(2)}) copy-start(bf16[256,512]{1,0:T(8,128)(2,1)} %fusion.48) | copy-start | bytes 786436
  212.0 4.5 %collective-permute-start.2 = (bf16[30,256]{1,0:T(8,128)(2,1)S(1)}, bf16[30,256]{1,0:T(8,128)(2,1)S(1)}, u32[]{:S(2)}, u32[]{:S(2)}) collective-permute-start(bf16[30,256]{1,0:T(8,128)(2,1)S(1)} %slice.1135), channel_id=1, source_target_pairs={{0,8},{8,16},{16,24},{1,9},{9,17},{17,25},{2,10},{10,18},{18,26},{... | collective-permute-start | bytes 46088 | tf_op jit(solution)/shard_map/ppermute | solution.py:12
Sparse Core Ops, SparseCore 0:
  9.2 29.4 all-gather.6
  65.9 24.0 all-gather.8
  93.4 28.0 all-gather.10
  148.6 24.0 all-gather.12
  176.1 28.0 all-gather.14
  231.2 24.0 all-gather.16
where the time goes:
time: 268 us; the launch traced here: 265 us
  waiting for transfers between devices  166 us (62%)
  blocking collectives  37.7 us (14%)
  matrix products  26.8 us (10%)
  between operations  13.7 us (5%)
  other arithmetic  13.3 us (5%)
  starting transfers between devices  4.21 us (2%)
  local copies, waits for them, and re-layouts  3.88 us (1%)
    all_gather x3, waiting for transfers between devices, on_device(): whole_rows = lax.all_gather(current, 'tp', axis=1, tiled=True)  83.1 us
    all_gather x3, waiting for transfers between devices, on_device(): lax.all_gather(hidden, 'tp', axis=1, tiled=True)  72.4 us
    psum x3, blocking collectives, on_device(): lax.psum((jnp.sum(convolved, axis=1), jnp.sum(convolved * convolved, axis...  37.7 us
    dot_general x6, matrix products, against(): lax.dot_general(left, right, (((1,), (1,)), ((), ())), preferred_element_...  16.8 us
    dot_general x3, matrix products, project_out(): return jnp.dot(block_in, out_matrix, preferred_element_type=jnp.float32)  9.99 us
    ppermute x3, waiting for transfers between devices, passed_along(): return lax.ppermute(shard, axis, pairs)  9.47 us
    reduce_sum x3, other arithmetic, on_device(): jnp.mean(whole_float * whole_float, axis=1, keepdims=True) + EPSILON  6.25 us
  transfers between devices with their start and end apart: 9, of which 9 were waited for; matrix products, arithmetic and copies ran while one was open for 2% of the time, Pallas kernels for 0%

commit v1 on v0

--- a/solution.py
+++ b/solution.py
@@ -1,6 +1,10 @@
+import functools
+
 import jax
 import jax.numpy as jnp
 from jax import lax
+from jax.experimental import pallas as pl
+from jax.experimental.pallas import tpu as pltpu
 from jax.sharding import PartitionSpec as P
 
 EPSILON = 1e-06
@@ -80,9 +84,381 @@
     return current
 
 
+LANES = 128
+SUBLANES = 8
+MESH = pl.DeviceIdType.MESH
+
+
+def flipped(index, bit):
+    return index + bit - 2 * bit * ((index // bit) % 2)
+
+
+def fused_kernel(
+    sp_count,
+    tp_count,
+    stream_ref,
+    gain_ref,
+    value_ref,
+    gate_ref,
+    kernel_ref,
+    bias_ref,
+    chan_gain_ref,
+    chan_shift_ref,
+    out_weight_ref,
+    result_ref,
+    cur_buf,
+    hid_buf,
+    weights,
+    out_weights,
+    gain32,
+    acc,
+    squares,
+    padded,
+    conv,
+    gated_buf,
+    halo,
+    stat_buf,
+    cur_recv,
+    cur_send,
+    hid_recv,
+    hid_send,
+    stat_recv,
+    stat_send,
+    halo_recv,
+    halo_send,
+    weight_sem,
+    stream_sem,
+):
+    sp = lax.axis_index("sp")
+    me = lax.axis_index("tp")
+    layers, taps, local_channels = kernel_ref.shape
+    rows, local_width = stream_ref.shape
+    width = local_width * tp_count
+    channels = local_channels * tp_count
+    half = rows // 2
+    halo_rows = halo.shape[1]
+    skip = halo_rows - (taps - 1)
+    pc, px, py = flipped(me, 1), flipped(me, 2), flipped(me, 4)
+    diag = flipped(px, 4)
+
+    def weight_copies(layer):
+        return (
+            pltpu.make_async_copy(
+                value_ref.at[layer],
+                weights.at[layer, pl.ds(0, local_channels)],
+                weight_sem.at[0, layer],
+            ),
+            pltpu.make_async_copy(
+                gate_ref.at[layer],
+                weights.at[layer, pl.ds(local_channels, local_channels)],
+                weight_sem.at[1, layer],
+            ),
+            pltpu.make_async_copy(
+                out_weight_ref.at[layer], out_weights.at[layer], weight_sem.at[2, layer]
+            ),
+        )
+
+    own_copy = pltpu.make_async_copy(stream_ref, cur_buf.at[me], stream_sem)
+    own_copy.start()
+    for layer in range(layers):
+        for copy in weight_copies(layer):
+            copy.start()
+
+    barrier = pltpu.get_barrier_semaphore()
+    for ahead in range(1, tp_count):
+        pl.semaphore_signal(
+            barrier,
+            inc=1,
+            device_id=(sp, lax.rem(me + ahead, tp_count)),
+            device_id_type=MESH,
+        )
+
+    around = (1, sp_count - 1) if sp_count > 1 else ()
+    for ahead in around:
+        pl.semaphore_signal(
+            barrier,
+            inc=1,
+            device_id=(lax.rem(sp + ahead, sp_count), me),
+            device_id_type=MESH,
+        )
+
+    for layer in range(layers):
+        gain32[layer] = gain_ref[layer : layer + 1].astype(jnp.float32)
+    own_copy.wait()
+    pl.semaphore_wait(barrier, tp_count - 1 + len(around))
+
+    def gather(buf, send, recv, consume):
+        def copy(slot, part, to, at):
+            piece = buf.at[slot, pl.ds(part * half, half)]
+            return pltpu.make_async_remote_copy(
+                src_ref=piece,
+                dst_ref=piece,
+                send_sem=send.at[at],
+                recv_sem=recv.at[slot, part],
+                device_id=(sp, to),
+                device_id_type=MESH,
+            )
+
+        started = []
+
+        def go(slot, part, to):
+            one = copy(slot, part, to, len(started))
+            one.start()
+            started.append(one)
+
+        def arrived(slot, part):
+            copy(slot, part, pc, 0).wait_recv()
+
+        go(me, 0, px)
+        go(me, 1, py)
+        go(me, 1, px)
+        go(me, 0, py)
+        go(me, 0, pc)
+        go(me, 1, pc)
+        consume(me, True)
+        arrived(pc, 0)
+        arrived(pc, 1)
+        consume(pc, False)
+        arrived(px, 0)
+        go(px, 0, py)
+        go(px, 0, pc)
+        arrived(py, 1)
+        go(py, 1, px)
+        go(py, 1, pc)
+        arrived(px, 1)
+        go(px, 1, pc)
+        arrived(py, 0)
+        go(py, 0, pc)
+        consume(px, False)
+        consume(py, False)
+        for slot in (flipped(pc, 2), flipped(pc, 4)):
+            arrived(slot, 0)
+            arrived(slot, 1)
+            consume(slot, False)
+        arrived(diag, 0)
+        go(diag, 0, pc)
+        arrived(diag, 1)
+        go(diag, 1, pc)
+        consume(diag, False)
+        last = flipped(diag, 1)
+        arrived(last, 0)
+        arrived(last, 1)
+        consume(last, False)
+        for one in started:
+            one.wait_send()
+
+    def row(ref, layer):
+        picked = ref[0:1]
+        for at in range(1, layers):
+            picked = jnp.where(layer == at, ref[at : at + 1], picked)
+        return picked
+
+    def one_layer(layer, carry):
+        value_copy, gate_copy, out_copy = weight_copies(layer)
+        value_copy.wait()
+        gate_copy.wait()
+
+        def consume_current(slot, first):
+            at = pl.multiple_of(slot * local_width, LANES)
+            block = cur_buf[slot].astype(jnp.float32)
+            squared = block * block
+            partial = squared[:, :LANES]
+            for lane in range(LANES, local_width, LANES):
+                partial = partial + squared[:, lane : lane + LANES]
+            gained = (block * gain32[layer, :, pl.ds(at, local_width)]).astype(jnp.bfloat16)
+            product = against(gained, weights[layer, :, pl.ds(at, local_width)])
+            if first:
+                squares[...] = partial
+                acc[...] = product
+            else:
+                squares[...] += partial
+                acc[...] += product
+
+        gather(cur_buf, cur_send, cur_recv, consume_current)
+
+        scale = lax.rsqrt(jnp.sum(squares[...], axis=1, keepdims=True) / width + EPSILON)
+        gated = (
+            acc[:, :local_channels]
+            * scale
+            * jax.nn.sigmoid(acc[:, local_channels:] * scale)
+        ).astype(jnp.bfloat16)
+        gated_buf[...] = gated[rows - halo_rows :]
+
+        def halo_copy(to):
+            return pltpu.make_async_remote_copy(
+                src_ref=gated_buf,
+                dst_ref=halo.at[layer],
+                send_sem=halo_send,
+                recv_sem=halo_recv.at[layer],
+                device_id=(to, me),
+                device_id_type=MESH,
+            )
+
+        @pl.when(sp < sp_count - 1)
+        def _():
+            halo_copy(sp + 1).start()
+
+        padded[pl.ds(halo_rows, rows)] = gated.astype(jnp.float32)
+
+        @pl.when(sp == 0)
+        def _():
+            padded[pl.ds(0, halo_rows)] = jnp.zeros((halo_rows, local_channels), jnp.float32)
+
+        tile = min(64, rows)
+        bias = row(bias_ref, layer)
+
+        def convolve(first_row):
+            for lane in range(0, local_channels, LANES):
+                total = jnp.broadcast_to(bias[:, lane : lane + LANES], (tile, LANES))
+                for tap in range(taps):
+                    total = total + kernel_ref[layer, tap : tap + 1, lane : lane + LANES] * padded[
+                        first_row + skip + tap : first_row + skip + tap + tile, lane : lane + LANES
+                    ]
+                conv[first_row : first_row + tile, lane : lane + LANES] = total
+
+        for first_row in range(tile, rows, tile):
+            convolve(first_row)
+
+        @pl.when(sp > 0)
+        def _():
+            halo_copy(sp - 1).wait_recv()
+            padded[pl.ds(0, halo_rows)] = halo[layer].astype(jnp.float32)
+
+        convolve(0)
+
+        convolved = conv[...]
+        lanes = lax.broadcasted_iota(jnp.int32, (rows, LANES), 1)
+        total = jnp.sum(convolved, axis=1, keepdims=True)
+        total_squared = jnp.sum(convolved * convolved, axis=1, keepdims=True)
+        both = jnp.where(lanes == 0, total, jnp.where(lanes == 1, total_squared, 0.0))
+        stat_buf[me] = both.T[:SUBLANES]
+
+        def stat_copy(slot, to, at):
+            return pltpu.make_async_remote_copy(
+                src_ref=stat_buf.at[slot],
+                dst_ref=stat_buf.at[slot],
+                send_sem=stat_send.at[at],
+                recv_sem=stat_recv.at[slot],
+                device_id=(sp, to),
+                device_id_type=MESH,
+            )
+
+        peers = [diag, flipped(diag, 1), px, py, flipped(px, 1), flipped(py, 1), pc]
+        sent = [stat_copy(me, peer, at) for at, peer in enumerate(peers)]
+        for one in sent:
+            one.start()
+        for peer in peers[::-1]:
+            stat_copy(peer, peer, 0).wait_recv()
+        summed = stat_buf[0]
+        for slot in range(1, tp_count):
+            summed = summed + stat_buf[slot]
+        summed = jnp.concatenate(
+            [summed, jnp.zeros((LANES - SUBLANES, rows), jnp.float32)], axis=0
+        ).T
+        centre = summed[:, 0:1] / channels
+        spread = summed[:, 1:2] / channels - centre * centre
+        normal_out = (convolved - centre) * lax.rsqrt(spread + EPSILON) * row(
+            chan_gain_ref, layer
+        ) + row(chan_shift_ref, layer)
+        hid_buf[me] = (normal_out / (1.0 + jnp.exp(-normal_out))).astype(jnp.bfloat16)
+        for one in sent:
+            one.wait_send()
+
+        @pl.when(sp < sp_count - 1)
+        def _():
+            halo_copy(sp + 1).wait_send()
+
+        out_copy.wait()
+
+        def consume_hidden(slot, first):
+            at = pl.multiple_of(slot * local_channels, LANES)
+            product = jnp.dot(
+                hid_buf[slot],
+                out_weights[layer, pl.ds(at, local_channels)],
+                preferred_element_type=jnp.float32,
+            )
+            if first:
+                acc[:, :local_width] = product
+            else:
+                acc[:, :local_width] += product
+
+        gather(hid_buf, hid_send, hid_recv, consume_hidden)
+        cur_buf[me] = (cur_buf[me].astype(jnp.float32) + acc[:, :local_width]).astype(jnp.bfloat16)
+        return carry
+
+    lax.fori_loop(0, layers, one_layer, 0)
+    result_ref[...] = cur_buf[me]
+
+
+def fused(
+    sp_count,
+    tp_count,
+    stream,
+    norm_gain,
+    value_weight,
+    gate_weight,
+    kernel,
+    kernel_bias,
+    chan_gain,
+    chan_shift,
+    out_weight,
+):
+    layers, taps, local_channels = kernel.shape
+    rows, local_width = stream.shape
+    halo_rows = -(-(taps - 1) // 16) * 16
+    any_space = pl.BlockSpec(memory_space=pl.ANY)
+    vmem = pl.BlockSpec(memory_space=pltpu.VMEM)
+    dma = pltpu.SemaphoreType.DMA
+    return pl.pallas_call(
+        functools.partial(fused_kernel, sp_count, tp_count),
+        out_shape=jax.ShapeDtypeStruct((rows, local_width), jnp.bfloat16),
+        in_specs=[any_space, vmem, any_space, any_space, vmem, vmem, vmem, vmem, any_space],
+        out_specs=vmem,
+        scratch_shapes=[
+            pltpu.VMEM((tp_count, rows, local_width), jnp.bfloat16),
+            pltpu.VMEM((tp_count, rows, local_channels), jnp.bfloat16),
+            pltpu.VMEM((layers, 2 * local_channels, local_width * tp_count), jnp.bfloat16),
+            pltpu.VMEM((layers,) + out_weight.shape[1:], jnp.bfloat16),
+            pltpu.VMEM((layers, 1, local_width * tp_count), jnp.float32),
+            pltpu.VMEM((rows, max(2 * local_channels, local_width)), jnp.float32),
+            pltpu.VMEM((rows, LANES), jnp.float32),
+            pltpu.VMEM((halo_rows + rows, local_channels), jnp.float32),
+            pltpu.VMEM((rows, local_channels), jnp.float32),
+            pltpu.VMEM((halo_rows, local_channels), jnp.bfloat16),
+            pltpu.VMEM((layers, halo_rows, local_channels), jnp.bfloat16),
+            pltpu.VMEM((tp_count, SUBLANES, rows), jnp.float32),
+            dma((tp_count, 2)),
+            dma((14,)),
+            dma((tp_count, 2)),
+            dma((14,)),
+            dma((tp_count,)),
+            dma((tp_count,)),
+            dma((layers,)),
+            dma,
+            dma((3, layers)),
+            dma,
+        ],
+        compiler_params=pltpu.CompilerParams(
+            collective_id=0, has_side_effects=True, vmem_limit_bytes=60 * 1024 * 1024
+        ),
+    )(
+        stream,
+        norm_gain,
+        value_weight,
+        gate_weight,
+        kernel,
+        kernel_bias,
+        chan_gain,
+        chan_shift,
+        out_weight,
+    )
+
+
 def solution(mesh):
+    cube = mesh.shape["tp"] == 2**3
+    body = functools.partial(fused, mesh.shape["sp"], mesh.shape["tp"]) if cube else on_device
     return jax.shard_map(
-        on_device,
+        body,
         mesh=mesh,
         in_specs=(
             P("sp", "tp"),

time: 268 us -> 91.2 us (0.34)
  waiting for transfers between devices: 166 us -> 0 us
  Pallas kernels: 0 us -> 89.4 us
  blocking collectives: 37.7 us -> 0 us
  matrix products: 26.8 us -> 0 us
  between operations: 13.7 us -> 0.01 us
  other arithmetic: 13.3 us -> 0 us
  starting transfers between devices: 4.21 us -> 0 us
    all_gather x6 -> x0, waiting for transfers between devices: 156 us -> none  [the longest x3 83.1 us: on_device(): whole_rows = lax.all_gather(current, 'tp', axis=1, tiled=True)]
    pallas_call x0 -> x1, Pallas kernels: none -> 89.4 us  [fused(): pl.pallas_call(functools.partial(fused_kernel, sp_count, tp_count), out_s...]
    psum x3 -> x0, blocking collectives: 37.7 us -> none  [on_device(): lax.psum((jnp.sum(convolved, axis=1), jnp.sum(convolved * convolved, axis...]
    dot_general x9 -> x0, matrix products: 26.8 us -> none  [the longest x6 16.8 us: against(): lax.dot_general(left, right, (((1,), (1,)), ((), ())), preferred_element_...]
    reduce_sum x6 -> x0, other arithmetic: 9.85 us -> none  [the longest x3 6.25 us: on_device(): jnp.mean(whole_float * whole_float, axis=1, keepdims=True) + EPSILON]
    ppermute x3 -> x0, waiting for transfers between devices: 9.47 us -> none  [passed_along(): return lax.ppermute(shard, axis, pairs)]
    ppermute x3 -> x0, starting transfers between devices: 4.01 us -> none  [passed_along(): return lax.ppermute(shard, axis, pairs)]
    slice x11 -> x0, local copies, waits for them, and re-layouts: 3.84 us -> none  [the longest x5 2.2 us: on_device(): kernel_now[tap_at][None, :]]
  transfers between devices with their start and end apart: 9 -> 0, of which waited for: 9 -> 0; matrix products, arithmetic and copies ran while one was open for 2% -> 0% of each run, Pallas kernels for 0% -> 0%
where the time goes in v1:
time: 91.2 us; the launch traced here: 91.1 us
  Pallas kernels  89.4 us (98%)
  local copies, waits for them, and re-layouts  1.67 us (2%)
    pallas_call x1, Pallas kernels, fused(): pl.pallas_call(functools.partial(fused_kernel, sp_count, tp_count), out_s...  89.4 us

profile of v1, /device:TPU:25, one launch (start us, length us, event | category | flops | bytes accessed | tf_op | source)
XLA Modules:
  0.0 91.1 jit_solution(10532744755991222825)
XLA Ops:
  0.0 89.4 %shard_map.91 = bf16[256,512]{1,0:T(8,128)(2,1)} custom-call(bf16[256,512]{1,0:T(8,128)(2,1)} %stream_ref.1, bf16[3,4096]{1,0:T(4,128)(2,1)} %gain_ref.1, bf16[3,256,4096]{2,1,0:T(8,128)(2,1)} %value_ref.1, bf16[3,256,4096]{2,1,0:T(8,128)(2,1)} %gate_ref.1, f32[3,31,256]{2,1,0:T(8,128)} %kernel_ref.1, f32[3,256]{1,0:T(4,128)} %bias_ref.1, ...), custom_call_target="tpu_custom_call" | custom-call | tf_op jit(solution)/shard_map/pallas_call | solution.py:412
  89.4 1.7 %copy.11 = bf16[256,512]{1,0:T(8,128)(2,1)} copy(bf16[256,512]{1,0:T(8,128)(2,1)} %shard_map.91) | data formatting | bytes 524288

commit v2 on v1

--- a/solution.py
+++ b/solution.py
@@ -118,12 +118,15 @@
     gated_buf,
     halo,
     stat_buf,
+    par_buf,
     cur_recv,
     cur_send,
     hid_recv,
     hid_send,
     stat_recv,
     stat_send,
+    par_recv,
+    par_send,
     halo_recv,
     halo_send,
     weight_sem,
@@ -136,6 +139,7 @@
     width = local_width * tp_count
     channels = local_channels * tp_count
     half = rows // 2
+    piece_rows = half // 2
     halo_rows = halo.shape[1]
     skip = halo_rows - (taps - 1)
     pc, px, py = flipped(me, 1), flipped(me, 2), flipped(me, 4)
@@ -187,65 +191,93 @@
     own_copy.wait()
     pl.semaphore_wait(barrier, tp_count - 1 + len(around))
 
-    def gather(buf, send, recv, consume):
-        def copy(slot, part, to, at):
-            piece = buf.at[slot, pl.ds(part * half, half)]
+    peers = [diag, flipped(diag, 1), px, py, flipped(px, 1), flipped(py, 1), pc]
+
+    def small_copies(buf, send, recv):
+        def copy(slot, to, at):
+            return pltpu.make_async_remote_copy(
+                src_ref=buf.at[slot],
+                dst_ref=buf.at[slot],
+                send_sem=send.at[at],
+                recv_sem=recv.at[slot],
+                device_id=(sp, to),
+                device_id_type=MESH,
+            )
+
+        sent = [copy(me, peer, at) for at, peer in enumerate(peers)]
+        came = [copy(peer, peer, 0) for peer in peers[::-1]]
+        return sent, came
+
+    for layer in range(layers):
+        par_buf[me, layer : layer + 1] = chan_gain_ref[layer : layer + 1]
+        par_buf[me, layers + layer : layers + layer + 1] = chan_shift_ref[layer : layer + 1]
+
+    class Gather:
+        def __init__(self, buf, send, recv):
+            self.buf, self.send, self.recv = buf, send, recv
+
+        def copy(self, slot, part, to, at):
+            piece = self.buf.at[slot, pl.ds(part * piece_rows, piece_rows)]
             return pltpu.make_async_remote_copy(
                 src_ref=piece,
                 dst_ref=piece,
-                send_sem=send.at[at],
-                recv_sem=recv.at[slot, part],
+                send_sem=self.send.at[at],
+                recv_sem=self.recv.at[slot, part],
                 device_id=(sp, to),
                 device_id_type=MESH,
             )
 
-        started = []
-
-        def go(slot, part, to):
-            one = copy(slot, part, to, len(started))
-            one.start()
-            started.append(one)
-
-        def arrived(slot, part):
-            copy(slot, part, pc, 0).wait_recv()
-
-        go(me, 0, px)
-        go(me, 1, py)
-        go(me, 1, px)
-        go(me, 0, py)
-        go(me, 0, pc)
-        go(me, 1, pc)
-        consume(me, True)
-        arrived(pc, 0)
-        arrived(pc, 1)
-        consume(pc, False)
-        arrived(px, 0)
-        go(px, 0, py)
-        go(px, 0, pc)
-        arrived(py, 1)
-        go(py, 1, px)
-        go(py, 1, pc)
-        arrived(px, 1)
-        go(px, 1, pc)
-        arrived(py, 0)
-        go(py, 0, pc)
-        consume(px, False)
-        consume(py, False)
-        for slot in (flipped(pc, 2), flipped(pc, 4)):
-            arrived(slot, 0)
-            arrived(slot, 1)
-            consume(slot, False)
-        arrived(diag, 0)
-        go(diag, 0, pc)
-        arrived(diag, 1)
-        go(diag, 1, pc)
-        consume(diag, False)
-        last = flipped(diag, 1)
-        arrived(last, 0)
-        arrived(last, 1)
-        consume(last, False)
-        for one in started:
-            one.wait_send()
+        def first(self, h):
+            self.copy(me, 2 * h, px, 14 * h).start()
+            self.copy(me, 2 * h + 1, py, 14 * h + 1).start()
+            self.copy(me, 2 * h, pc, 14 * h + 2).start()
+            self.copy(me, 2 * h + 1, pc, 14 * h + 3).start()
+
+        def second(self, h):
+            self.copy(me, 2 * h + 1, px, 14 * h + 4).start()
+            self.copy(me, 2 * h, py, 14 * h + 5).start()
+
+        def arrived(self, slot, part):
+            self.copy(slot, part, pc, 0).wait_recv()
+
+        def half_arrived(self, slot, h):
+            self.arrived(slot, 2 * h)
+            self.arrived(slot, 2 * h + 1)
+
+        def relay_first(self, h):
+            self.arrived(px, 2 * h)
+            self.copy(px, 2 * h, py, 14 * h + 6).start()
+            self.copy(px, 2 * h, pc, 14 * h + 7).start()
+            self.arrived(py, 2 * h + 1)
+            self.copy(py, 2 * h + 1, px, 14 * h + 8).start()
+            self.copy(py, 2 * h + 1, pc, 14 * h + 9).start()
+
+        def relay_second(self, h):
+            self.arrived(px, 2 * h + 1)
+            self.copy(px, 2 * h + 1, pc, 14 * h + 10).start()
+            self.arrived(py, 2 * h)
+            self.copy(py, 2 * h, pc, 14 * h + 11).start()
+
+        def relay_third(self, h):
+            self.arrived(diag, 2 * h)
+            self.copy(diag, 2 * h, pc, 14 * h + 12).start()
+            self.arrived(diag, 2 * h + 1)
+            self.copy(diag, 2 * h + 1, pc, 14 * h + 13).start()
+
+        def all_sent(self):
+            for at in range(28):
+                self.copy(me, 0, pc, at).wait_send()
+
+    cur = Gather(cur_buf, cur_send, cur_recv)
+    hid = Gather(hid_buf, hid_send, hid_recv)
+    beyond = flipped(diag, 1), flipped(px, 1), flipped(py, 1)
+    cur.first(0)
+    cur.second(0)
+    par_sent, par_came = small_copies(par_buf, par_send, par_recv)
+    for one in par_sent:
+        one.start()
+    cur.first(1)
+    cur.second(1)
 
     def row(ref, layer):
         picked = ref[0:1]
@@ -274,7 +306,26 @@
                 squares[...] += partial
                 acc[...] += product
 
-        gather(cur_buf, cur_send, cur_recv, consume_current)
+        consume_current(me, True)
+        cur.relay_first(0)
+        cur.half_arrived(pc, 0)
+        cur.relay_first(1)
+        cur.half_arrived(pc, 1)
+        consume_current(pc, False)
+        cur.relay_second(0)
+        cur.relay_second(1)
+        consume_current(px, False)
+        consume_current(py, False)
+        for slot in beyond[1:]:
+            cur.half_arrived(slot, 0)
+            cur.half_arrived(slot, 1)
+            consume_current(slot, False)
+        cur.relay_third(0)
+        cur.relay_third(1)
+        consume_current(diag, False)
+        cur.half_arrived(beyond[0], 0)
+        cur.half_arrived(beyond[0], 1)
+        consume_current(beyond[0], False)
 
         scale = lax.rsqrt(jnp.sum(squares[...], axis=1, keepdims=True) / width + EPSILON)
         gated = (
@@ -327,28 +378,26 @@
         convolve(0)
 
         convolved = conv[...]
+        hid_buf[me] = convolved.astype(jnp.bfloat16)
+        hid.first(0)
         lanes = lax.broadcasted_iota(jnp.int32, (rows, LANES), 1)
         total = jnp.sum(convolved, axis=1, keepdims=True)
         total_squared = jnp.sum(convolved * convolved, axis=1, keepdims=True)
         both = jnp.where(lanes == 0, total, jnp.where(lanes == 1, total_squared, 0.0))
         stat_buf[me] = both.T[:SUBLANES]
 
-        def stat_copy(slot, to, at):
-            return pltpu.make_async_remote_copy(
-                src_ref=stat_buf.at[slot],
-                dst_ref=stat_buf.at[slot],
-                send_sem=stat_send.at[at],
-                recv_sem=stat_recv.at[slot],
-                device_id=(sp, to),
-                device_id_type=MESH,
-            )
-
-        peers = [diag, flipped(diag, 1), px, py, flipped(px, 1), flipped(py, 1), pc]
-        sent = [stat_copy(me, peer, at) for at, peer in enumerate(peers)]
-        for one in sent:
+        stat_sent, stat_came = small_copies(stat_buf, stat_send, stat_recv)
+        for one in stat_sent:
             one.start()
-        for peer in peers[::-1]:
-            stat_copy(peer, peer, 0).wait_recv()
+        hid.second(0)
+        hid.first(1)
+        cur.all_sent()
+        out_copy.wait()
+        hid.relay_first(0)
+        hid.second(1)
+        hid.relay_first(1)
+        for one in stat_came:
+            one.wait_recv()
         summed = stat_buf[0]
         for slot in range(1, tp_count):
             summed = summed + stat_buf[slot]
@@ -357,33 +406,78 @@
         ).T
         centre = summed[:, 0:1] / channels
         spread = summed[:, 1:2] / channels - centre * centre
-        normal_out = (convolved - centre) * lax.rsqrt(spread + EPSILON) * row(
-            chan_gain_ref, layer
-        ) + row(chan_shift_ref, layer)
-        hid_buf[me] = (normal_out / (1.0 + jnp.exp(-normal_out))).astype(jnp.bfloat16)
-        for one in sent:
-            one.wait_send()
-
-        @pl.when(sp < sp_count - 1)
-        def _():
-            halo_copy(sp + 1).wait_send()
-
-        out_copy.wait()
-
-        def consume_hidden(slot, first):
+        steepness = lax.rsqrt(spread + EPSILON)
+
+        def consume_hidden(slot, h, first):
             at = pl.multiple_of(slot * local_channels, LANES)
+            here = slice(h * half, (h + 1) * half)
+            gain = par_buf[slot, 0:1]
+            shift = par_buf[slot, layers : layers + 1]
+            for other in range(1, layers):
+                gain = jnp.where(layer == other, par_buf[slot, other : other + 1], gain)
+                shift = jnp.where(
+                    layer == other, par_buf[slot, layers + other : layers + other + 1], shift
+                )
+            normal_out = (hid_buf[slot, here].astype(jnp.float32) - centre[here]) * steepness[
+                here
+            ] * gain + shift
+            hidden = (normal_out / (1.0 + jnp.exp(-normal_out))).astype(jnp.bfloat16)
             product = jnp.dot(
-                hid_buf[slot],
+                hidden,
                 out_weights[layer, pl.ds(at, local_channels)],
                 preferred_element_type=jnp.float32,
             )
             if first:
-                acc[:, :local_width] = product
+                acc[here, :local_width] = product
             else:
-                acc[:, :local_width] += product
-
-        gather(hid_buf, hid_send, hid_recv, consume_hidden)
-        cur_buf[me] = (cur_buf[me].astype(jnp.float32) + acc[:, :local_width]).astype(jnp.bfloat16)
+                acc[here, :local_width] += product
+
+        def finish(h):
+            for slot in beyond[1:]:
+                hid.half_arrived(slot, h)
+                consume_hidden(slot, h, False)
+            consume_hidden(diag, h, False)
+            hid.half_arrived(beyond[0], h)
+            consume_hidden(beyond[0], h, False)
+            here = slice(h * half, (h + 1) * half)
+            cur_buf[me, here] = (
+                cur_buf[me, here].astype(jnp.float32) + acc[here, :local_width]
+            ).astype(jnp.bfloat16)
+
+            @pl.when(layer < layers - 1)
+            def _():
+                cur.first(h)
+                cur.second(h)
+
+        @pl.when(layer == 0)
+        def _():
+            for one in par_came:
+                one.wait_recv()
+            for one in par_sent:
+                one.wait_send()
+
+        for h in range(2):
+            if h == 1:
+                hid.relay_third(1)
+            consume_hidden(me, h, True)
+            hid.half_arrived(pc, h)
+            consume_hidden(pc, h, False)
+            if h == 0:
+                hid.relay_second(0)
+                hid.relay_second(1)
+            consume_hidden(px, h, False)
+            consume_hidden(py, h, False)
+            if h == 0:
+                hid.relay_third(0)
+            finish(h)
+        for one in stat_sent:
+            one.wait_send()
+        hid.all_sent()
+
+        @pl.when(sp < sp_count - 1)
+        def _():
+            halo_copy(sp + 1).wait_send()
+
         return carry
 
     lax.fori_loop(0, layers, one_layer, 0)
@@ -406,6 +500,7 @@
     layers, taps, local_channels = kernel.shape
     rows, local_width = stream.shape
     halo_rows = -(-(taps - 1) // 16) * 16
+    par_rows = -(-2 * layers // SUBLANES) * SUBLANES
     any_space = pl.BlockSpec(memory_space=pl.ANY)
     vmem = pl.BlockSpec(memory_space=pltpu.VMEM)
     dma = pltpu.SemaphoreType.DMA
@@ -427,10 +522,13 @@
             pltpu.VMEM((halo_rows, local_channels), jnp.bfloat16),
             pltpu.VMEM((layers, halo_rows, local_channels), jnp.bfloat16),
             pltpu.VMEM((tp_count, SUBLANES, rows), jnp.float32),
-            dma((tp_count, 2)),
-            dma((14,)),
-            dma((tp_count, 2)),
-            dma((14,)),
+            pltpu.VMEM((tp_count, par_rows, local_channels), jnp.float32),
+            dma((tp_count, 4)),
+            dma((28,)),
+            dma((tp_count, 4)),
+            dma((28,)),
+            dma((tp_count,)),
+            dma((tp_count,)),
             dma((tp_count,)),
             dma((tp_count,)),
             dma((layers,)),

time: 91.2 us -> 79 us (0.87)
  Pallas kernels: 89.4 us -> 76.9 us
    pallas_call x1, Pallas kernels: 89.4 us -> 76.9 us  [fused(): pl.pallas_call(functools.partial(fused_kernel, sp_count, tp_count), out_s...]
where the time goes in v2:
time: 79 us; the launch traced here: 78.6 us
  Pallas kernels  76.9 us (97%)
  local copies, waits for them, and re-layouts  1.67 us (2%)
    pallas_call x1, Pallas kernels, fused(): pl.pallas_call(functools.partial(fused_kernel, sp_count, tp_count), out_s...  76.9 us
    unnamed x1, local copies, waits for them, and re-layouts  1.67 us

profile of v2, /device:TPU:25, one launch (start us, length us, event | category | flops | bytes accessed | tf_op | source)
XLA Modules:
  0.0 78.6 jit_solution(5312036278075028597)
XLA Ops:
  0.0 76.9 %shard_map.91 = bf16[256,512]{1,0:T(8,128)(2,1)} custom-call(bf16[256,512]{1,0:T(8,128)(2,1)} %stream_ref.1, bf16[3,4096]{1,0:T(4,128)(2,1)} %gain_ref.1, bf16[3,256,4096]{2,1,0:T(8,128)(2,1)} %value_ref.1, bf16[3,256,4096]{2,1,0:T(8,128)(2,1)} %gate_ref.1, f32[3,31,256]{2,1,0:T(8,128)} %kernel_ref.1, f32[3,256]{1,0:T(4,128)} %bias_ref.1, ...), custom_call_target="tpu_custom_call" | custom-call | tf_op jit(solution)/shard_map/pallas_call | solution.py:507
  76.9 1.7 %copy.11 = bf16[256,512]{1,0:T(8,128)(2,1)} copy(bf16[256,512]{1,0:T(8,128)(2,1)} %shard_map.91) | data formatting | bytes 524288
